TPU v7x, 32 devices: a whole 2x2x4 slice. The times are simulated.
32 devices in a mesh: grp: 2 (over x), ep: 8 (over z, y), tp: 2 (over core).
Axes of the slice: x: 2, y: 2, z: 4, core: 2. Of those that a mesh axis runs over, the one named last changes fastest.
Arguments:
- tokens: bfloat16 [8192, 2048], P(('grp', 'ep'), 'tp'), parts along dimension 0, may hold values from -6 to 6
- norm_gain: float32 [2048], replicated, may hold values from 0.1 to 1.9
- expert_ids: int32 [8192, 2], P(('grp', 'ep')), parts along dimension 0, may hold values from 0 to 7, all different within a row; in each aligned block of 512 rows (0 to 511, 512 to 1023, ...) at most 192 rows name the same one
- route_weights: float32 [8192, 2], P(('grp', 'ep')), parts along dimension 0, may hold values from 0.1 to 1
- gate_weight: bfloat16 [8, 2048, 512], P('ep', None, 'tp'), may hold values from -0.125 to 0.125
- up_weight: bfloat16 [8, 2048, 512], P('ep', None, 'tp'), may hold values from -0.125 to 0.125
- down_weight: bfloat16 [8, 512, 2048], P('ep', None, 'tp'), may hold values from -0.25 to 0.25
Outputs:
- mixed: bfloat16 [8192, 2048], P(('grp', 'ep'), 'tp'), parts along dimension 0
There are 2 independent parts, one for each index of `grp`. A program takes and returns all parts, laid end to end along the dimension named above; an argument that names none is the same for every part. Nothing has to cross between parts.
Inputs may be any that keep to these rules, and one draw needn't show every extreme that they name: `expert_ids`: each token names 2 different experts. Among the 512 tokens of one index of ep (aligned blocks of rows) at most 192 name the same expert, and in some block some expert is named by exactly 192 of them.
All inputs are finite; a program needn't handle non-finite values.
Results may differ from a plain program's by a relative error of at most 0.007.
Values may be sent and summed in bfloat16 or wider, within the bound.
A program may use at most 64 MiB of HBM per device.

v0:
```python
import jax
import jax.numpy as jnp
from jax import lax
from jax.sharding import PartitionSpec as P


def normalize(rows, norm_gain):
    xf = rows.astype(jnp.float32)
    scale = lax.rsqrt(jnp.mean(xf * xf, axis=-1, keepdims=True) + 1e-06)
    return (xf * scale * norm_gain[None, :]).astype(jnp.bfloat16)


def on_device(tokens, norm_gain, expert_ids, route_weights, gate_weight, up_weight, down_weight):
    tok_rows, half = tokens.shape
    width = half * lax.axis_size("tp")
    experts = lax.axis_size("ep")
    top = expert_ids.shape[1]
    capacity = max(2, (3 * tok_rows * top + 2 * experts - 1) // (2 * experts))
    flat = expert_ids.reshape(-1)
    onehot = (flat[:, None] == jnp.arange(experts, dtype=jnp.int32)[None, :]).astype(jnp.int32)
    earlier = jnp.cumsum(onehot, axis=0) - onehot
    slot = jnp.sum(earlier * onehot, axis=-1)
    position = flat * capacity + slot
    owner = jnp.arange(flat.shape[0], dtype=jnp.int32) // top
    w_gate = gate_weight[0]
    w_up = up_weight[0]
    w_down = down_weight[0]
    send = jnp.zeros((experts * capacity, half), jnp.bfloat16).at[position].set(tokens[owner])
    send = send.reshape(experts, capacity, half)
    received = lax.all_to_all(send, "ep", split_axis=0, concat_axis=0, tiled=True)
    sources = received.shape[0]
    count = received.shape[1]
    whole_rows = lax.all_gather(received, "tp", axis=2, tiled=True)
    rows = normalize(whole_rows.reshape(sources * count, width), norm_gain)
    gate = jnp.dot(rows, w_gate, preferred_element_type=jnp.float32)
    upper = jnp.dot(rows, w_up, preferred_element_type=jnp.float32)
    hidden = (jax.nn.silu(gate) * upper).astype(jnp.bfloat16)
    result = jnp.dot(
        lax.all_gather(hidden, "tp", axis=1, tiled=True), w_down, preferred_element_type=jnp.float32
    )
    result = result.astype(jnp.bfloat16).reshape(sources, count, half)
    back = lax.all_to_all(result, "ep", split_axis=0, concat_axis=0, tiled=True)
    picked = back.reshape(experts * capacity, half)[position].astype(jnp.float32)
    picked = picked * route_weights.reshape(-1)[:, None]
    return jnp.sum(picked.reshape(tok_rows, top, half), axis=1).astype(jnp.bfloat16)


def solution(mesh):
    in_specs = (
        P(("grp", "ep"), "tp"),
        P(),
        P(("grp", "ep"), None),
        P(("grp", "ep"), None),
        P("ep", None, "tp"),
        P("ep", None, "tp"),
        P("ep", None, "tp"),
    )
    out_specs = P(("grp", "ep"), "tp")
    return jax.shard_map(
        on_device, mesh=mesh, in_specs=in_specs, out_specs=out_specs, check_vma=False
    )
```

profile of v0, /device:TPU:0, one launch (start us, length us, event | category | flops | bytes accessed | tf_op | source)
XLA Modules:
  0.0 251.1 jit_solution(1036192993760471310)
XLA Ops:
  6.5 0.9 copy.14
  7.5 0.2 eq.29
  7.6 0.2 eq.25
  7.8 0.7 broadcast_multiply_fusion
  8.5 2.3 reduce-window.6
  10.8 0.3 slice_reduce_fusion
  11.1 0.2 reduce-window.9
  11.5 0.2 mul.61
  11.7 14.8 %scatter_custom_fusion = bf16[1536,1024]{1,0:T(8,128)(2,1)} fusion(s32[1024]{0:T(1024)S(1)} %bitcast.43, bf16[512,1024]{1,0:T(8,128)(2,1)S(1)} %copy-done, s32[1024]{0:T(1024)S(1)} %broadcast_clamp_fusion.1, bf16[]{:T(256)} %constant.29.clone.1), kind=kCustom, calls=%fused_computation.12 | custom fusion | bytes 3145730 | tf_op jit(solution)/shard_map/scatter | solution.py:28
  26.5 78.1 %all_to_all.10 = bf16[8,192,1024]{2,1,0:T(8,128)(2,1)} all-to-all(bf16[8,192,1024]{2,1,0:T(8,128)(2,1)} %bitcast.38), channel_id=1, replica_groups=mesh['grp'=2,'ep'=8,'tp'=2] {'ep'}, dimensions={0} | all-to-all | bytes 6291456 | tf_op jit(solution)/shard_map/all_to_all | solution.py:30
  104.6 0.2 all-gather.5.cloned.1.call-start
  104.9 15.7 %all-gather.3.cloned.1.call-done = bf16[8,192,2048]{2,1,0:T(8,128)(2,1)} async-done(((bf16[8,192,1024]{2,1,0:T(8,128)(2,1)}), bf16[8,192,2048]{2,1,0:T(8,128)(2,1)}) %all-gather.3.cloned.1.call-update) | async-done | bytes 6291472 | tf_op jit(solution)/shard_map/all_gather | solution.py:33
  120.6 4.2 %fusion = f32[8,192]{1,0:T(8,128)S(1)} fusion(bf16[8,192,2048]{2,1,0:T(8,128)(2,1)} %all-gather.3.cloned.1.call-done), kind=kLoop, calls=%fused_computation.5 | loop fusion | flops 9435648 | bytes 6297600 | tf_op jit(solution)/shard_map/reduce_sum | solution.py:9
  124.8 0.3 copy-done.1
  125.2 1.5 fusion.2
  126.7 1.9 fusion.9
  128.6 3.0 %fusion.3 = bf16[1536,256]{1,0:T(8,128)(2,1)} fusion(bf16[1536,2048]{1,0:T(8,128)(2,1)S(1)} %bitcast.40, f32[1536,256]{1,0:T(8,128)S(1)} %fusion.9, bf16[1,2048,256]{2,1,0:T(8,128)(2,1)S(1)} %copy-done.5), kind=kOutput, calls=%fused_computation.11 | convolution fusion | flops 1612972032 | bytes 9699328 | tf_op jit(solution)/shard_map/dot_general | solution.py:36
  131.5 10.8 %all-gather.5.cloned.1.call-done = bf16[1536,512]{1,0:T(8,128)(2,1)} async-done(((bf16[1536,256]{1,0:T(8,128)(2,1)}), bf16[1536,512]{1,0:T(8,128)(2,1)}) %all-gather.5.cloned.1.call-update) | async-done | bytes 1572880 | tf_op jit(solution)/shard_map/all_gather | solution.py:39
  142.3 4.9 %convolution_convert_fusion = bf16[1536,1024]{1,0:T(8,128)(2,1)} fusion(bf16[1536,512]{1,0:T(8,128)(2,1)} %all-gather.5.cloned.1.call-done, bf16[1,512,1024]{2,1,0:T(8,128)(2,1)S(1)} %copy-done.6), kind=kOutput, calls=%fused_computation.9 | convolution fusion | flops 1612185600 | bytes 5767168 | tf_op jit(solution)/shard_map/dot_general | solution.py:38
  147.2 5.9 %all-to-all-start.1 = ((bf16[8,192,1024]{2,1,0:T(8,128)(2,1)}), bf16[8,192,1024]{2,1,0:T(8,128)(2,1)}, u32[]{:S(2)}, u32[]{:S(2)}) async-start(bf16[8,192,1024]{2,1,0:T(8,128)(2,1)} %bitcast.41), calls=%async_computation.1 | async-start | bytes 6291456 | tf_op jit(solution)/shard_map/all_to_all | solution.py:42
  153.3 71.1 %all-to-all-done.1 = bf16[8,192,1024]{2,1,0:T(8,128)(2,1)} async-done(((bf16[8,192,1024]{2,1,0:T(8,128)(2,1)}), bf16[8,192,1024]{2,1,0:T(8,128)(2,1)}, u32[]{:S(2)}, u32[]{:S(2)}) %all-to-all-start.1) | async-done | bytes 3145760 | tf_op jit(solution)/shard_map/all_to_all | solution.py:42
  224.4 7.3 %gather_fusion = bf16[1024,1024]{1,0:T(8,128)(2,1)S(1)} fusion(bf16[1536,1024]{1,0:T(8,128)(2,1)} %bitcast.10, s32[1024]{0:T(1024)S(1)} %broadcast_clamp_fusion), kind=kCustom, calls=%fused_computation.1 | custom fusion | bytes 4198400 | tf_op jit(solution)/shard_map/gather | solution.py:43
  231.7 4.0 %reshape.146 = f32[512,2,1024]{2,1,0:T(2,128)} reshape(bf16[1024,1024]{1,0:T(8,128)(2,1)S(1)} %gather_fusion) | data formatting | bytes 6291456 | tf_op jit(solution)/shard_map/convert_element_type | solution.py:43
  235.7 8.6 %multiply_reduce_fusion = bf16[512,1024]{1,0:T(8,128)(2,1)} fusion(f32[512,2,1024]{2,1,0:T(2,128)} %reshape.146, f32[512,2]{1,0:T(8,128)S(1)} %copy.16), kind=kLoop, calls=%fused_computation.8 | loop fusion | flops 1572864 | bytes 5246976 | tf_op jit(solution)/shard_map/reduce_sum | solution.py:45
  (26 shorter events, 0.5 us)
Async XLA Ops:
  6.5 5.2 %copy-start = (bf16[512,1024]{1,0:T(8,128)(2,1)S(1)}, bf16[512,1024]{1,0:T(8,128)(2,1)}, u32[]{:S(2)}) copy-start(bf16[512,1024]{1,0:T(8,128)(2,1)} %param.7) | copy-start | bytes 3145732
  6.5 114.0 %all-gather.3.cloned.1.call-start = ((), (), s32[]{:S(2)}) async-start(), calls=%async_computation.2 | async-start | bytes 9437184 | tf_op jit(solution)/shard_map/all_gather | solution.py:33
  104.6 20.2 %copy-start.2 = (f32[2048]{0:T(1024)S(1)}, f32[2048]{0:T(1024)}, u32[]{:S(2)}) copy-start(f32[2048]{0:T(1024)} %param.8) | copy-start | bytes 24580
  104.6 37.7 %all-gather.5.cloned.1.call-start = ((), (), s32[]{:S(2)}) async-start(), calls=%async_computation.3 | async-start | bytes 2359296 | tf_op jit(solution)/shard_map/all_gather | solution.py:39
  120.6 4.6 %copy-start.1 = (bf16[8,192,2048]{2,1,0:T(8,128)(2,1)S(1)}, bf16[8,192,2048]{2,1,0:T(8,128)(2,1)}, u32[]{:S(2)}) copy-start(bf16[8,192,2048]{2,1,0:T(8,128)(2,1)} %all-gather.3.cloned.1.call-done) | copy-start | bytes 18874372
  125.2 1.5 copy-start.4
  126.7 1.9 copy-start.5
  128.5 13.8 %copy-start.6 = (bf16[1,512,1024]{2,1,0:T(8,128)(2,1)S(1)}, bf16[1,512,1024]{2,1,0:T(8,128)(2,1)}, u32[]{:S(2)}) copy-start(bf16[1,512,1024]{2,1,0:T(8,128)(2,1)} %param.13) | copy-start | bytes 3145732
  147.2 6.0 %copy-start.3 = (f32[512,2]{0,1:T(2,128)S(1)}, f32[512,2]{0,1:T(2,128)}, u32[]{:S(2)}) copy-start(f32[512,2]{0,1:T(2,128)} %param.10) | copy-start | bytes 12292
  147.2 77.2 %all-to-all-start.1 = ((bf16[8,192,1024]{2,1,0:T(8,128)(2,1)}), bf16[8,192,1024]{2,1,0:T(8,128)(2,1)}, u32[]{:S(2)}, u32[]{:S(2)}) async-start(bf16[8,192,1024]{2,1,0:T(8,128)(2,1)} %bitcast.41), calls=%async_computation.1 | async-start | bytes 6291456 | tf_op jit(solution)/shard_map/all_to_all | solution.py:42
Sparse Core Ops, SparseCore 0:
  104.8 15.7 all-gather.2
  131.7 10.6 all-gather.4
where the time goes:
time: 252 us; the launch traced here: 251 us
  waiting for transfers between devices  97.6 us (39%)
  blocking collectives  78.1 us (31%)
  local copies, waits for them, and re-layouts  28.4 us (11%)
  other arithmetic  17.6 us (7%)
  between operations  13.6 us (5%)
  matrix products  9.71 us (4%)
  starting transfers between devices  6.17 us (2%)
    all_to_all x1, blocking collectives, on_device(): lax.all_to_all(send, 'ep', split_axis=0, concat_axis=0, tiled=True)  78.1 us
    all_to_all x1, waiting for transfers between devices, on_device(): back = lax.all_to_all(result, 'ep', split_axis=0, concat_axis=0, tiled=True)  71.1 us
    all_gather x1, waiting for transfers between devices, on_device(): whole_rows = lax.all_gather(received, 'tp', axis=2, tiled=True)  15.7 us
    scatter x1, local copies, waits for them, and re-layouts, on_device(): jnp.zeros((experts * capacity, half), jnp.bfloat16).at[position]  14.8 us
    all_gather x1, waiting for transfers between devices, on_device(): lax.all_gather(hidden, 'tp', axis=1, tiled=True)  10.8 us
    reduce_sum x1, other arithmetic, on_device(): jnp.sum(picked.reshape(tok_rows, top, half), axis=1).astype(jnp.bfloat16)  8.58 us
    gather x1, local copies, waits for them, and re-layouts, on_device(): back.reshape(experts * capacity, half)[position].astype(jnp.float32)  7.27 us
    all_to_all x1, starting transfers between devices, on_device(): back = lax.all_to_all(result, 'ep', split_axis=0, concat_axis=0, tiled=True)  5.95 us
  transfers between devices with their start and end apart: 3, of which 3 were waited for; matrix products, arithmetic and copies ran while one was open for 0% of the time, Pallas kernels for 0%

commit v1 on v0

--- a/solution.py
+++ b/solution.py
@@ -1,7 +1,14 @@
+import functools
+
 import jax
 import jax.numpy as jnp
 from jax import lax
+from jax.experimental import pallas as pl
+from jax.experimental.pallas import tpu as pltpu
 from jax.sharding import PartitionSpec as P
+
+MESH = pl.DeviceIdType.MESH
+COLS = 2
 
 
 def normalize(rows, norm_gain):
@@ -10,7 +17,7 @@
     return (xf * scale * norm_gain[None, :]).astype(jnp.bfloat16)
 
 
-def on_device(tokens, norm_gain, expert_ids, route_weights, gate_weight, up_weight, down_weight):
+def sparse_form(tokens, norm_gain, expert_ids, route_weights, gate_weight, up_weight, down_weight):
     tok_rows, half = tokens.shape
     width = half * lax.axis_size("tp")
     experts = lax.axis_size("ep")
@@ -45,6 +52,347 @@
     return jnp.sum(picked.reshape(tok_rows, top, half), axis=1).astype(jnp.bfloat16)
 
 
+def line_kernel(
+    length, tok_ref, gain_ref, route_ref, gate_in, up_in, down_in, out_ref,
+    raw, x, wt, wg, wu, wd, hid, acc, part, from_low, from_high, fin, outs,
+    swap_s, swap_r, loc, own_s, own_r, wy_s, wy_r, wx_s, wx_r, p1_s, p1_r, p2_s, p2_r,
+    up_s, up_r, dn_s, dn_r, upt_s, upt_r, dnt_s, dnt_r, ru_s, ru_r, rd_s, rd_r, fin_s, fin_r,
+):
+    f32 = jnp.float32
+    g, ep, c = lax.axis_index("grp"), lax.axis_index("ep"), lax.axis_index("tp")
+    z, y = ep // COLS, ep % COLS
+    last = length - 1
+    mate, across, beside = {"tp": 1 - c}, {"grp": 1 - g}, {"ep": z * COLS + 1 - y}
+    above, below = {"ep": ep + COLS}, {"ep": ep - COLS}
+    rows, half = raw.shape[1], raw.shape[2]
+    piece = rows // 2
+
+    def remote(src, dst, ss, rs, dev):
+        return pltpu.make_async_remote_copy(
+            src_ref=src, dst_ref=dst, send_sem=ss, recv_sem=rs, device_id=dev, device_id_type=MESH
+        )
+
+    barrier = pltpu.get_barrier_semaphore()
+    for dev in (mate, across, beside):
+        pl.semaphore_signal(barrier, inc=1, device_id=dev, device_id_type=MESH)
+
+    @pl.when(z < last)
+    def _():
+        pl.semaphore_signal(barrier, inc=1, device_id=above, device_id_type=MESH)
+
+    @pl.when(z > 0)
+    def _():
+        pl.semaphore_signal(barrier, inc=1, device_id=below, device_id_type=MESH)
+
+    ends = jnp.where(z == 0, 1, 0) + jnp.where(z == last, 1, 0)
+    pl.semaphore_wait(barrier, 5 - ends)
+
+    swap = remote(tok_ref.at[1 - c], raw.at[c], swap_s, swap_r, mate)
+    swap.start()
+
+    mats = ((gate_in, wg), (up_in, wu), (down_in, wd))
+    chunks = []
+    for m in range(3):
+        quarter = mats[m][0].shape[0] // 4
+        for u in range(2):
+            chunks.append((m, u, quarter))
+
+    def cut(portion, u, quarter):
+        return pl.ds(pl.multiple_of((portion * 2 + u) * quarter, quarter), quarter)
+
+    def send_y(t):
+        m, u, q = chunks[t]
+        src, dst = mats[m]
+        return remote(src.at[cut(g, u, q)], dst.at[1, c, cut(g, u, q)], wy_s.at[t], wy_r.at[t], beside)
+
+    def send_x(t, portion):
+        m, u, q = chunks[t]
+        buf = mats[m][1].at[1, c, cut(portion, u, q)]
+        return remote(buf, buf, wx_s.at[t], wx_r.at[t], across)
+
+    def send_mate(t, portion, half_of, ss, rs):
+        m, u, q = chunks[t]
+        buf = mats[m][1].at[1, half_of, cut(portion, u, q)]
+        return remote(buf, buf, ss.at[t], rs.at[t], mate)
+
+    for t in range(6):
+        send_y(t).start()
+    own = []
+    for m in range(3):
+        src, dst = mats[m]
+        own.append(remote(src, dst.at[0, c], own_s.at[m], own_r.at[m], mate))
+    local = [pltpu.make_async_copy(mats[m][0], mats[m][1].at[0, c], loc.at[m]) for m in range(3)]
+
+    for copy in own + local:
+        copy.start()
+    wt[z] = route_ref[...]
+    swap.wait_recv()
+    step = rows // 8
+
+    def norm(i, carry):
+        at = pl.ds(pl.multiple_of(i * step, step), step)
+        a = tok_ref[c, at].astype(f32)
+        b = raw[1 - c, at].astype(f32)
+        total = jnp.sum(a * a, axis=-1, keepdims=True) + jnp.sum(b * b, axis=-1, keepdims=True)
+        scale = lax.rsqrt(total / (2 * half) + 1e-06)
+        x[z, c, at] = (a * scale * gain_ref[c]).astype(x.dtype)
+        x[z, 1 - c, at] = (b * scale * gain_ref[1 - c]).astype(x.dtype)
+        return carry
+
+    lax.fori_loop(0, 8, norm, 0)
+
+    def rise(b):
+        return (
+            remote(x.at[b], x.at[b], up_s.at[b], up_r.at[b], above),
+            remote(wt.at[b], wt.at[b], upt_s.at[b], upt_r.at[b], above),
+        )
+
+    def fall(b):
+        return (
+            remote(x.at[b], x.at[b], dn_s.at[b], dn_r.at[b], below),
+            remote(wt.at[b], wt.at[b], dnt_s.at[b], dnt_r.at[b], below),
+        )
+
+    @pl.when(z < last)
+    def _():
+        for copy in rise(z):
+            copy.start()
+
+    @pl.when(z > 0)
+    def _():
+        for copy in fall(z):
+            copy.start()
+
+    def hand_on(k):
+        @pl.when(z >= k)
+        def _():
+            for copy in rise(z - k):
+                copy.wait_recv()
+
+            @pl.when(z < last)
+            def _():
+                for copy in rise(z - k):
+                    copy.start()
+
+        @pl.when(z + k <= last)
+        def _():
+            for copy in fall(z + k):
+                copy.wait_recv()
+
+            @pl.when(z > 0)
+            def _():
+                for copy in fall(z + k):
+                    copy.start()
+
+    def got_y(t):
+        m, u, q = chunks[t]
+        send_y(t).wait_recv()
+        send_x(t, g).start()
+        send_mate(t, g, c, p1_s, p1_r).start()
+
+    def got_x(t):
+        send_x(t, 1 - g).wait_recv()
+        send_mate(t, 1 - g, c, p2_s, p2_r).start()
+
+    for t in range(6):
+        got_y(t)
+        if t >= 1:
+            got_x(t - 1)
+        if t == 3:
+            hand_on(1)
+    got_x(5)
+    for t in range(6):
+        send_mate(t, g, 1 - c, p1_s, p1_r).wait_recv()
+        send_mate(t, 1 - g, 1 - c, p2_s, p2_r).wait_recv()
+    for m in range(3):
+        local[m].wait()
+        own[m].wait_recv()
+
+    def experts_on(b):
+        columns = wt[b].T
+        lane = lax.broadcasted_iota(jnp.int32, columns.shape, 1)
+        for s in range(2):
+            expert = z * COLS + (y if s == 0 else 1 - y)
+            weight = jnp.sum(jnp.where(lane == expert, columns, 0.0), axis=1, keepdims=True)
+            for h in range(2):
+                both = []
+                for w in (wg, wu):
+                    both.append(
+                        jnp.dot(x[b, 0], w[s, h, :half], preferred_element_type=f32)
+                        + jnp.dot(x[b, 1], w[s, h, half:], preferred_element_type=f32)
+                    )
+                gate, upper = both
+                silu = gate * (0.5 * (1.0 + jnp.tanh(0.5 * gate)))
+                wide = gate.shape[1]
+                hid[:, h * wide:(h + 1) * wide] = (silu * upper).astype(hid.dtype)
+            for f in range(2):
+                got = jnp.dot(hid[...], wd[s, f], preferred_element_type=f32)
+                got = got.astype(jnp.bfloat16).astype(f32) * weight
+                if s == 0:
+                    acc[f] = got
+                else:
+                    got = acc[f] + got
+                    acc[f] = got
+                    part[b, f] = got.astype(part.dtype)
+
+    def place(j):
+        return (1 - c if j < 2 else c), pl.ds((j % 2) * piece, piece)
+
+    def sum_up(b, j):
+        f, at = place(j)
+        return remote(part.at[b, f, at], from_low.at[b, f, at], ru_s.at[b, j], ru_r.at[b, j], above)
+
+    def sum_down(b, j):
+        f, at = place(j)
+        return remote(part.at[b, f, at], from_high.at[b, f, at], rd_s.at[b, j], rd_r.at[b, j], below)
+
+    def stage(k, carry):
+        @pl.when(k > 1)
+        def _():
+            hand_on(k)
+
+        def one(i, inner):
+            b = jnp.where(k > last, z, jnp.where(i == 0, z - k, z + k))
+
+            @pl.when((b >= 0) & (b <= last) & ((k <= last) | (i == 0)))
+            def _():
+                experts_on(b)
+            return inner
+
+        lax.fori_loop(0, 2, one, 0)
+
+        for j in range(4):
+            f, at = place(j)
+
+            @pl.when((z < k) & (k <= last))
+            def _():
+                @pl.when(z > 0)
+                def _():
+                    sum_up(k, j).wait_recv()
+                    part[k, f, at] = (part[k, f, at].astype(f32) + from_low[k, f, at].astype(f32)).astype(part.dtype)
+                sum_up(k, j).start()
+
+            low = last - k
+
+            @pl.when((z > low) & (k <= last))
+            def _():
+                @pl.when(z < last)
+                def _():
+                    sum_down(low, j).wait_recv()
+                    part[low, f, at] = (
+                        part[low, f, at].astype(f32) + from_high[low, f, at].astype(f32)
+                    ).astype(part.dtype)
+                sum_down(low, j).start()
+        return carry
+
+    lax.fori_loop(1, length + 1, stage, 0)
+
+    def give(r):
+        at = pl.ds(r * piece, piece)
+        return remote(fin.at[at], outs.at[c, at], fin_s.at[r], fin_r.at[r], mate)
+
+    for j in range(4):
+        f, at = place(j)
+
+        @pl.when(z > 0)
+        def _():
+            sum_up(z, j).wait_recv()
+            acc[f, at] = acc[f, at] + from_low[z, f, at].astype(f32)
+
+        @pl.when(z < last)
+        def _():
+            sum_down(z, j).wait_recv()
+            acc[f, at] = acc[f, at] + from_high[z, f, at].astype(f32)
+
+        if j < 2:
+            fin[at] = acc[f, at].astype(fin.dtype)
+            give(j).start()
+        else:
+            out_ref[c, at] = acc[f, at].astype(out_ref.dtype)
+    for r in range(2):
+        at = pl.ds(r * piece, piece)
+        give(r).wait_recv()
+        out_ref[1 - c, at] = outs[1 - c, at]
+
+    swap.wait_send()
+    for copy in own:
+        copy.wait_send()
+    for t in range(6):
+        send_y(t).wait_send()
+        send_x(t, g).wait_send()
+        send_mate(t, g, c, p1_s, p1_r).wait_send()
+        send_mate(t, 1 - g, c, p2_s, p2_r).wait_send()
+    for r in range(2):
+        give(r).wait_send()
+    for b in range(length):
+        @pl.when((z >= b) & (z < last))
+        def _():
+            for copy in rise(b):
+                copy.wait_send()
+
+        @pl.when((z <= b) & (z > 0))
+        def _():
+            for copy in fall(b):
+                copy.wait_send()
+
+        @pl.when(z < b)
+        def _():
+            for j in range(4):
+                sum_up(b, j).wait_send()
+
+        @pl.when(z > b)
+        def _():
+            for j in range(4):
+                sum_down(b, j).wait_send()
+
+
+def line_form(tokens, norm_gain, expert_ids, route_weights, gate_weight, up_weight, down_weight):
+    tok_rows, half = tokens.shape
+    experts = lax.axis_size("ep")
+    length = experts // COLS
+    rows = tok_rows // 2
+    mine = lax.axis_index("tp")
+    bf16, f32 = jnp.bfloat16, jnp.float32
+    chosen = expert_ids[None] == jnp.arange(experts, dtype=jnp.int32)[:, None, None]
+    route = jnp.sum(jnp.where(chosen, route_weights[None], 0.0), axis=-1)
+    route = lax.dynamic_slice_in_dim(route, mine * rows, rows, axis=1)
+    gate, up, down = gate_weight[0], up_weight[0], down_weight[0]
+    dma, vmem = pltpu.SemaphoreType.DMA, pltpu.VMEM
+    block = (length, 2, rows, half)
+    sems = []
+    for shape in (
+        (1,), (3,), (6,), (6,), (6,), (6,), (length,), (length,), (length,), (length,), (length, 4), (length, 4), (2,)
+    ):
+        sems += [dma(shape), dma(shape)]
+    sems = [dma, dma, dma((3,))] + sems[2:]
+    out = pl.pallas_call(
+        functools.partial(line_kernel, length),
+        out_shape=jax.ShapeDtypeStruct((2, rows, half), bf16),
+        in_specs=[pl.BlockSpec(memory_space=vmem)] * 3 + [pl.BlockSpec(memory_space=pl.ANY)] * 3,
+        out_specs=pl.BlockSpec(memory_space=vmem),
+        scratch_shapes=[
+            vmem((2, rows, half), bf16),
+            vmem(block, bf16),
+            vmem((length, experts, rows), f32),
+            vmem((2, 2) + gate.shape, bf16),
+            vmem((2, 2) + up.shape, bf16),
+            vmem((2, 2) + down.shape, bf16),
+            vmem((rows, 2 * gate.shape[1]), bf16),
+            vmem((2, rows, half), f32),
+            vmem(block, bf16),
+            vmem(block, bf16),
+            vmem(block, bf16),
+            vmem((rows, half), bf16),
+            vmem((2, rows, half), bf16),
+        ]
+        + sems,
+        compiler_params=pltpu.CompilerParams(
+            collective_id=0, has_side_effects=True, vmem_limit_bytes=60 * 1024 * 1024
+        ),
+    )(tokens.reshape(2, rows, half), norm_gain.reshape(2, 1, half), route, gate, up, down)
+    return out.reshape(tok_rows, half)
+
+
 def solution(mesh):
     in_specs = (
         P(("grp", "ep"), "tp"),
@@ -56,6 +404,13 @@
         P("ep", None, "tp"),
     )
     out_specs = P(("grp", "ep"), "tp")
+    shape = mesh.shape
+
+    def on_device(tokens, norm_gain, expert_ids, *rest):
+        dense = shape["ep"] <= 4 * expert_ids.shape[1] and shape["ep"] % COLS == 0 and shape["ep"] > COLS
+        form = line_form if dense and shape["grp"] == 2 and shape["tp"] == 2 else sparse_form
+        return form(tokens, norm_gain, expert_ids, *rest)
+
     return jax.shard_map(
         on_device, mesh=mesh, in_specs=in_specs, out_specs=out_specs, check_vma=False
     )

time: 252 us -> 170 us (0.67)
  Pallas kernels: 0 us -> 167 us
  waiting for transfers between devices: 97.6 us -> 0 us
  blocking collectives: 78.1 us -> 0 us
  local copies, waits for them, and re-layouts: 28.4 us -> 3.57 us
  other arithmetic: 17.6 us -> 0.01 us
  between operations: 13.6 us -> 0.01 us
  matrix products: 9.71 us -> 0 us
  starting transfers between devices: 6.17 us -> 0 us
    pallas_call x0 -> x1, Pallas kernels: none -> 167 us  [line_form(): pl.pallas_call(functools.partial(line_kernel, length), out_shape=jax.Shap...]
    all_to_all x1 -> x0, blocking collectives: 78.1 us -> none  [on_device(): lax.all_to_all(send, 'ep', split_axis=0, concat_axis=0, tiled=True)]
    all_to_all x1 -> x0, waiting for transfers between devices: 71.1 us -> none  [on_device(): back = lax.all_to_all(result, 'ep', split_axis=0, concat_axis=0, tiled=True)]
    all_gather x2 -> x0, waiting for transfers between devices: 26.5 us -> none  [the longest x1 15.7 us: on_device(): whole_rows = lax.all_gather(received, 'tp', axis=2, tiled=True)]
    scatter x1 -> x0, local copies, waits for them, and re-layouts: 14.8 us -> none  [on_device(): jnp.zeros((experts * capacity, half), jnp.bfloat16).at[position]]
    reduce_sum x3 -> x1, other arithmetic: 12.8 us -> 0.01 us  [line_form(): route = jnp.sum(jnp.where(chosen, route_weights[None], 0.0), axis=-1)]
    dot_general x3 -> x0, matrix products: 9.71 us -> none  [the longest x1 4.89 us: on_device(): jnp.dot(lax.all_gather(hidden, 'tp', axis=1, tiled=True), w_down, preferr...]
    gather x1 -> x0, local copies, waits for them, and re-layouts: 7.27 us -> none  [on_device(): back.reshape(experts * capacity, half)[position].astype(jnp.float32)]
  transfers between devices with their start and end apart: 3 -> 0, of which waited for: 3 -> 0; matrix products, arithmetic and copies ran while one was open for 0% -> 0% of each run, Pallas kernels for 0% -> 0%
where the time goes in v1:
time: 170 us
  Pallas kernels  167 us (98%)
  local copies, waits for them, and re-layouts  3.57 us (2%)
    pallas_call x1, Pallas kernels, line_form(): pl.pallas_call(functools.partial(line_kernel, length), out_shape=jax.Shap...  167 us

profile of v1, /device:TPU:0, one launch (start us, length us, event | category | flops | bytes accessed | tf_op | source)
XLA Modules:
  0.0 170.2 jit_solution(2776432241668501320)
XLA Ops:
  0.0 0.0 copy-start.1
  0.0 0.0 copy-start
  0.0 0.7 copy-done.1
  0.7 0.0 copy-done
  0.7 0.6 constant_dynamic-slice_fusion.route_ref
  1.3 166.6 %shard_map.73 = bf16[2,256,1024]{2,1,0:T(8,128)(2,1)} custom-call(bf16[2,256,1024]{2,1,0:T(8,128)(2,1)} %bitcast.7, f32[2,1,1024]{2,1,0:T(1,128)} %bitcast.11, f32[8,256]{1,0:T(8,128)} %constant_dynamic-slice_fusion.route_ref, bf16[2048,256]{1,0:T(8,128)(2,1)} %bitcast.8, bf16[2048,256]{1,0:T(8,128)(2,1)} %bitcast.9, bf16[512,1024]{1,0:T(8,128)(2,1)} %bitcast.10), custom_call_target="tpu_custom_call" | custom-call | tf_op jit(solution)/shard_map/pallas_call | solution.py:368
  167.9 2.3 %copy.11 = bf16[512,1024]{1,0:T(8,128)(2,1)} copy(bf16[512,1024]{1,0:T(8,128)(2,1)} %bitcast.6) | data formatting | bytes 2097152
  (1 shorter events, 0.0 us)
Async XLA Ops:
  0.0 0.7 copy-start.1
  0.0 0.7 copy-start

commit v2 on v1

--- a/solution.py
+++ b/solution.py
@@ -9,6 +9,8 @@
 
 MESH = pl.DeviceIdType.MESH
 COLS = 2
+PARTS = 8
+CUTS = 4
 
 
 def normalize(rows, norm_gain):
@@ -65,7 +67,7 @@
     mate, across, beside = {"tp": 1 - c}, {"grp": 1 - g}, {"ep": z * COLS + 1 - y}
     above, below = {"ep": ep + COLS}, {"ep": ep - COLS}
     rows, half = raw.shape[1], raw.shape[2]
-    piece = rows // 2
+    piece = rows // (PARTS // 2)
 
     def remote(src, dst, ss, rs, dev):
         return pltpu.make_async_remote_copy(
@@ -93,12 +95,13 @@
     mats = ((gate_in, wg), (up_in, wu), (down_in, wd))
     chunks = []
     for m in range(3):
-        quarter = mats[m][0].shape[0] // 4
-        for u in range(2):
-            chunks.append((m, u, quarter))
-
-    def cut(portion, u, quarter):
-        return pl.ds(pl.multiple_of((portion * 2 + u) * quarter, quarter), quarter)
+        size = mats[m][0].shape[0] // (2 * CUTS)
+        for u in range(CUTS):
+            chunks.append((m, u, size))
+    amount = len(chunks)
+
+    def cut(portion, u, size):
+        return pl.ds(pl.multiple_of((portion * CUTS + u) * size, size), size)
 
     def send_y(t):
         m, u, q = chunks[t]
@@ -115,7 +118,7 @@
         buf = mats[m][1].at[1, half_of, cut(portion, u, q)]
         return remote(buf, buf, ss.at[t], rs.at[t], mate)
 
-    for t in range(6):
+    for t in range(amount):
         send_y(t).start()
     own = []
     for m in range(3):
@@ -194,14 +197,14 @@
         send_x(t, 1 - g).wait_recv()
         send_mate(t, 1 - g, c, p2_s, p2_r).start()
 
-    for t in range(6):
+    for t in range(amount):
         got_y(t)
         if t >= 1:
             got_x(t - 1)
-        if t == 3:
+        if t == 3 * amount // 4 - 1:
             hand_on(1)
-    got_x(5)
-    for t in range(6):
+    got_x(amount - 1)
+    for t in range(amount):
         send_mate(t, g, 1 - c, p1_s, p1_r).wait_recv()
         send_mate(t, 1 - g, 1 - c, p2_s, p2_r).wait_recv()
     for m in range(3):
@@ -236,7 +239,7 @@
                     part[b, f] = got.astype(part.dtype)
 
     def place(j):
-        return (1 - c if j < 2 else c), pl.ds((j % 2) * piece, piece)
+        return (1 - c if j < PARTS // 2 else c), pl.ds((j % (PARTS // 2)) * piece, piece)
 
     def sum_up(b, j):
         f, at = place(j)
@@ -245,6 +248,28 @@
     def sum_down(b, j):
         f, at = place(j)
         return remote(part.at[b, f, at], from_high.at[b, f, at], rd_s.at[b, j], rd_r.at[b, j], below)
+
+    def wave_up(b, j, side):
+        f, at = place(j)
+
+        @pl.when(side & (z < b) & (b <= last))
+        def _():
+            @pl.when(z > 0)
+            def _():
+                sum_up(b, j).wait_recv()
+                part[b, f, at] = (part[b, f, at].astype(f32) + from_low[b, f, at].astype(f32)).astype(part.dtype)
+            sum_up(b, j).start()
+
+    def wave_down(b, j, side):
+        f, at = place(j)
+
+        @pl.when(side & (z > b) & (b >= 0))
+        def _():
+            @pl.when(z < last)
+            def _():
+                sum_down(b, j).wait_recv()
+                part[b, f, at] = (part[b, f, at].astype(f32) + from_high[b, f, at].astype(f32)).astype(part.dtype)
+            sum_down(b, j).start()
 
     def stage(k, carry):
         @pl.when(k > 1)
@@ -261,28 +286,13 @@
 
         lax.fori_loop(0, 2, one, 0)
 
-        for j in range(4):
-            f, at = place(j)
-
-            @pl.when((z < k) & (k <= last))
-            def _():
-                @pl.when(z > 0)
-                def _():
-                    sum_up(k, j).wait_recv()
-                    part[k, f, at] = (part[k, f, at].astype(f32) + from_low[k, f, at].astype(f32)).astype(part.dtype)
-                sum_up(k, j).start()
-
-            low = last - k
-
-            @pl.when((z > low) & (k <= last))
-            def _():
-                @pl.when(z < last)
-                def _():
-                    sum_down(low, j).wait_recv()
-                    part[low, f, at] = (
-                        part[low, f, at].astype(f32) + from_high[low, f, at].astype(f32)
-                    ).astype(part.dtype)
-                sum_down(low, j).start()
+        for j in range(PARTS + 1):
+            if j < PARTS:
+                wave_up(k, j, z < length // 2)
+                wave_down(last - k, j, z >= length // 2)
+            if j > 0:
+                wave_down(last - k, j - 1, z < length // 2)
+                wave_up(k, j - 1, z >= length // 2)
         return carry
 
     lax.fori_loop(1, length + 1, stage, 0)
@@ -291,7 +301,7 @@
         at = pl.ds(r * piece, piece)
         return remote(fin.at[at], outs.at[c, at], fin_s.at[r], fin_r.at[r], mate)
 
-    for j in range(4):
+    for j in range(PARTS):
         f, at = place(j)
 
         @pl.when(z > 0)
@@ -304,12 +314,12 @@
             sum_down(z, j).wait_recv()
             acc[f, at] = acc[f, at] + from_high[z, f, at].astype(f32)
 
-        if j < 2:
+        if j < PARTS // 2:
             fin[at] = acc[f, at].astype(fin.dtype)
             give(j).start()
         else:
             out_ref[c, at] = acc[f, at].astype(out_ref.dtype)
-    for r in range(2):
+    for r in range(PARTS // 2):
         at = pl.ds(r * piece, piece)
         give(r).wait_recv()
         out_ref[1 - c, at] = outs[1 - c, at]
@@ -317,12 +327,12 @@
     swap.wait_send()
     for copy in own:
         copy.wait_send()
-    for t in range(6):
+    for t in range(amount):
         send_y(t).wait_send()
         send_x(t, g).wait_send()
         send_mate(t, g, c, p1_s, p1_r).wait_send()
         send_mate(t, 1 - g, c, p2_s, p2_r).wait_send()
-    for r in range(2):
+    for r in range(PARTS // 2):
         give(r).wait_send()
     for b in range(length):
         @pl.when((z >= b) & (z < last))
@@ -337,12 +347,12 @@
 
         @pl.when(z < b)
         def _():
-            for j in range(4):
+            for j in range(PARTS):
                 sum_up(b, j).wait_send()
 
         @pl.when(z > b)
         def _():
-            for j in range(4):
+            for j in range(PARTS):
                 sum_down(b, j).wait_send()
 
 
@@ -359,9 +369,10 @@
     gate, up, down = gate_weight[0], up_weight[0], down_weight[0]
     dma, vmem = pltpu.SemaphoreType.DMA, pltpu.VMEM
     block = (length, 2, rows, half)
+    cuts, sums = (3 * CUTS,), (length, PARTS)
     sems = []
     for shape in (
-        (1,), (3,), (6,), (6,), (6,), (6,), (length,), (length,), (length,), (length,), (length, 4), (length, 4), (2,)
+        (1,), (3,), cuts, cuts, cuts, cuts, (length,), (length,), (length,), (length,), sums, sums, (PARTS // 2,)
     ):
         sems += [dma(shape), dma(shape)]
     sems = [dma, dma, dma((3,))] + sems[2:]

time: 170 us -> 137 us (0.81)
  Pallas kernels: 167 us -> 133 us
    pallas_call x1, Pallas kernels: 167 us -> 133 us  [line_form(): pl.pallas_call(functools.partial(line_kernel, length), out_shape=jax.Shap...]
where the time goes in v2:
time: 137 us
  Pallas kernels  133 us (97%)
  local copies, waits for them, and re-layouts  3.57 us (3%)
    pallas_call x1, Pallas kernels, line_form(): pl.pallas_call(functools.partial(line_kernel, length), out_shape=jax.Shap...  133 us
    unnamed x5, local copies, waits for them, and re-layouts  2.96 us

profile of v2, /device:TPU:0, one launch (start us, length us, event | category | flops | bytes accessed | tf_op | source)
XLA Modules:
  0.0 137.0 jit_solution(9823071714552479036)
XLA Ops:
  0.0 0.0 copy-start.1
  0.0 0.0 copy-start
  0.0 0.7 copy-done.1
  0.7 0.0 copy-done
  0.7 0.6 constant_dynamic-slice_fusion.route_ref
  1.3 133.4 %shard_map.73 = bf16[2,256,1024]{2,1,0:T(8,128)(2,1)} custom-call(bf16[2,256,1024]{2,1,0:T(8,128)(2,1)} %bitcast.7, f32[2,1,1024]{2,1,0:T(1,128)} %bitcast.11, f32[8,256]{1,0:T(8,128)} %constant_dynamic-slice_fusion.route_ref, bf16[2048,256]{1,0:T(8,128)(2,1)} %bitcast.8, bf16[2048,256]{1,0:T(8,128)(2,1)} %bitcast.9, bf16[512,1024]{1,0:T(8,128)(2,1)} %bitcast.10), custom_call_target="tpu_custom_call" | custom-call | tf_op jit(solution)/shard_map/pallas_call | solution.py:379
  134.7 2.3 %copy.11 = bf16[512,1024]{1,0:T(8,128)(2,1)} copy(bf16[512,1024]{1,0:T(8,128)(2,1)} %bitcast.6) | data formatting | bytes 2097152
  (1 shorter events, 0.0 us)
Async XLA Ops:
  0.0 0.7 copy-start.1
  0.0 0.7 copy-start
